TPU v7x, 32 devices: a whole 2x2x4 slice. The times are simulated.
32 devices in a mesh: ra: 4 (over z), cb: 4 (over y, x), dp: 2 (over core).
Axes of the slice: x: 2, y: 2, z: 4, core: 2. Of those that a mesh axis runs over, the one named last changes fastest.
Arguments:
- tokens: bfloat16 [2, 512, 4096], P('dp', None, 'ra'), may hold values from -80 to 80
- pre_gain: float32 [4096], P('ra'), may hold values from 0.1 to 1.9
- w_gate: bfloat16 [4096, 11264], P('ra', 'cb'), may hold values from -0.09375 to 0.09375
- w_up: bfloat16 [4096, 11264], P('ra', 'cb'), may hold values from -0.09375 to 0.09375
- conv_gate: float32 [3, 11264], P(None, 'cb'), may hold values from -3.5 to 3.5
- conv_up: float32 [3, 11264], P(None, 'cb'), may hold values from -3.5 to 3.5
- w_down: bfloat16 [11264, 4096], P('cb', 'ra'), may hold values from -2 to 2
- post_gain: float32 [4096], P('ra'), may hold values from 0.1 to 1.9
Outputs:
- mixed: bfloat16 [2, 512, 4096], P('dp', None, 'ra')
All inputs are finite; a program needn't handle non-finite values.
Results may differ from a plain program's by a relative error of at most 0.0064.
Values may be sent and summed in bfloat16 or wider, within the bound.
A program may use at most 128 MiB of HBM per device.

v0:
```python
import jax
import jax.numpy as jnp
from jax import lax
from jax.sharding import PartitionSpec as P

epsilon = 1e-06
residual_scale = 0.125


def convolve(field, tap_weights):
    zero_col = jnp.zeros((field.shape[0], 1), jnp.float32)
    before = jnp.concatenate([zero_col, field[:, :-1]], axis=1)
    later_cols = jnp.concatenate([field[:, 1:], zero_col], axis=1)
    return (
        tap_weights[0][:, None] * before
        + tap_weights[1][:, None] * field
        + tap_weights[2][:, None] * later_cols
    )


def local(tokens, pre_gain, w_gate, w_up, conv_gate, conv_up, w_down, post_gain):
    ra_count = lax.axis_size("ra")
    dim_full = tokens.shape[2] * ra_count
    values = tokens[0].astype(jnp.float32)
    local_sq = jnp.sum(values * values, axis=1)
    total_sq = lax.psum(local_sq, "ra")
    in_scale = lax.rsqrt(total_sq / dim_full + epsilon)
    weighted = (values * pre_gain).astype(jnp.bfloat16)
    gate_cols, up_cols = (
        lax.all_to_all(w_gate, "ra", split_axis=1, concat_axis=0, tiled=True),
        lax.all_to_all(w_up, "ra", split_axis=1, concat_axis=0, tiled=True),
    )
    own_units = gate_cols.shape[1]
    piece = lax.all_gather(weighted, "ra", axis=1, tiled=True)
    dims = (((0,), (1,)), ((), ()))
    gate_sum = lax.dot_general(gate_cols, piece, dims, preferred_element_type=jnp.float32)
    up_sum = lax.dot_general(up_cols, piece, dims, preferred_element_type=jnp.float32)
    offset_units = lax.axis_index("ra") * own_units
    taps_gate = lax.dynamic_slice_in_dim(conv_gate, offset_units, own_units, 1)
    taps_up = lax.dynamic_slice_in_dim(conv_up, offset_units, own_units, 1)
    gate_lin = gate_sum * in_scale[None, :]
    up_lin = up_sum * in_scale[None, :]
    hidden = (
        jax.nn.gelu(convolve(gate_lin, taps_gate), approximate=True) * convolve(up_lin, taps_up)
    ).astype(jnp.bfloat16)
    partial_value = lax.dot_general(
        lax.all_gather(hidden, "ra", axis=0, tiled=True),
        w_down,
        (((0,), (0,)), ((), ())),
        preferred_element_type=jnp.float32,
    )
    branch = lax.psum(partial_value, "cb")
    post_sq = lax.psum(jnp.sum(branch * branch, axis=1), "ra")
    post_scale = lax.rsqrt(post_sq / dim_full + epsilon)
    mixed = residual_scale * values + branch * post_scale[:, None] * post_gain
    return mixed.astype(jnp.bfloat16)[None]


def solution(mesh):
    in_specs = (
        P("dp", None, "ra"),
        P("ra"),
        P("ra", "cb"),
        P("ra", "cb"),
        P(None, "cb"),
        P(None, "cb"),
        P("cb", "ra"),
        P("ra"),
    )
    out_specs = P("dp", None, "ra")
    return jax.shard_map(local, mesh=mesh, in_specs=in_specs, out_specs=out_specs, check_vma=False)
```

profile of v0, /device:TPU:0, one launch (start us, length us, event | category | flops | bytes accessed | tf_op | source)
XLA Modules:
  0.0 532.4 jit_solution(12061142635943834656)
XLA Ops:
  6.5 8.3 %copy.11 = bf16[1024,2816]{0,1:T(8,128)(2,1)} copy(bf16[1024,2816]{1,0:T(8,128)(2,1)} %param.11) | data formatting | bytes 11534336 | tf_op args[3]
  14.8 6.3 %all-to-all-start.1 = ((bf16[1024,4,704]{0,2,1:T(8,128)(2,1)}), bf16[1024,4,704]{0,2,1:T(8,128)(2,1)}, u32[]{:S(2)}, u32[]{:S(2)}) async-start(bf16[1024,4,704]{0,2,1:T(8,128)(2,1)} %bitcast.26), calls=%async_computation.1 | async-start | bytes 11534336 | tf_op jit(solution)/shard_map/all_to_all | solution.py:31
  21.1 8.3 %copy.9 = bf16[1024,2816]{0,1:T(8,128)(2,1)} copy(bf16[1024,2816]{1,0:T(8,128)(2,1)} %param.10) | data formatting | bytes 11534336 | tf_op args[2]
  29.5 119.1 %all-to-all-done.1 = bf16[1024,4,704]{0,2,1:T(8,128)(2,1)} async-done(((bf16[1024,4,704]{0,2,1:T(8,128)(2,1)}), bf16[1024,4,704]{0,2,1:T(8,128)(2,1)}, u32[]{:S(2)}, u32[]{:S(2)}) %all-to-all-start.1) | async-done | bytes 5767200 | tf_op jit(solution)/shard_map/all_to_all | solution.py:31
  148.6 0.0 copy-start.2
  148.6 0.0 copy-start.3
  148.6 5.3 all-to-all-start
  153.9 0.0 all-gather.3.cloned.1.call-start
  154.0 0.0 copy-done.2
  154.0 0.0 copy-done.3
  154.0 1.3 fusion.3
  155.2 0.0 all-gather.3.cloned.1.call-update
  155.3 0.0 all-gather.5.cloned.1.call-start
  155.3 1.0 dynamic-slice_reduce_fusion.2
  156.3 163.7 %psum.21 = f32[512]{0:T(512)S(1)} all-reduce(f32[512]{0:T(512)S(1)} %get-tuple-element.15), channel_id=1, replica_groups=mesh['ra'=4,'cb'=4,'dp'=2] {'ra'}, use_global_device_ids=true, to_apply=%region_1.0 | all-reduce | flops 512 | bytes 4096 | tf_op jit(solution)/shard_map/psum | solution.py:26
  320.0 6.1 %copy.14 = bf16[4,88,8,1024]{3,2,0,1:T(8,128)(2,1)} copy(bf16[4,88,8,1024]{3,2,1,0:T(8,128)(2,1)} %bitcast.11) | data formatting | bytes 11534336 | tf_op jit(solution)/shard_map/all_to_all | solution.py:31
  326.1 22.0 %all-to-all-done = bf16[1024,4,704]{0,2,1:T(8,128)(2,1)} async-done(((bf16[1024,4,704]{0,2,1:T(8,128)(2,1)}), bf16[1024,4,704]{0,2,1:T(8,128)(2,1)}, u32[]{:S(2)}, u32[]{:S(2)}) %all-to-all-start) | async-done | bytes 5767200 | tf_op jit(solution)/shard_map/all_to_all | solution.py:30
  348.1 6.1 %copy.13 = bf16[4,88,8,1024]{3,2,0,1:T(8,128)(2,1)} copy(bf16[4,88,8,1024]{3,2,1,0:T(8,128)(2,1)} %bitcast.9) | data formatting | bytes 11534336 | tf_op jit(solution)/shard_map/all_to_all | solution.py:30
  354.3 0.0 all-gather.3.cloned.1.call-done
  354.3 0.0 copy-start.1
  354.3 0.0 copy-start.5
  354.3 6.6 %fusion.4 = f32[704,512]{1,0:T(8,128)S(1)} fusion(bf16[512,4096]{1,0:T(8,128)(2,1)} %all-gather.3.cloned.1.call-done, bf16[4096,704]{0,1:T(8,128)(2,1)} %bitcast.27, f32[512]{0:T(512)S(1)} %add_rsqrt_fusion.1), kind=kOutput, calls=%fused_computation.10 | convolution fusion | flops 2953150464 | bytes 11405312 | tf_op jit(solution)/shard_map/dot_general | solution.py:37
  360.9 0.0 copy-done.1
  360.9 0.1 copy-done.5
  361.0 3.2 fusion.5
  364.2 1.0 fusion.16
  365.2 2.8 fusion.14
  368.0 0.0 all-gather.5.cloned.1.call-update
  368.0 0.0 all-reduce.6.cloned.1.call-start
  368.1 66.4 %all-gather.5.cloned.1.call-done = bf16[2816,512]{1,0:T(8,128)(2,1)} async-done(((bf16[704,512]{1,0:T(8,128)(2,1)}), bf16[2816,512]{1,0:T(8,128)(2,1)}) %all-gather.5.cloned.1.call-update) | async-done | bytes 2883600 | tf_op jit(solution)/shard_map/all_gather | solution.py:47
  434.5 8.0 %fusion.18 = f32[512,1024]{1,0:T(8,128)} fusion(bf16[2816,512]{1,0:T(8,128)(2,1)} %all-gather.5.cloned.1.call-done, bf16[2816,1024]{1,0:T(8,128)(2,1)} %param.14), kind=kOutput, calls=%fused_computation.33 | convolution fusion | flops 2952790016 | bytes 10747904 | tf_op jit(solution)/shard_map/dot_general | solution.py:46
  442.5 0.0 all-reduce.6.cloned.1.call-update
  442.5 0.0 copy-start.4
  442.5 68.3 %all-reduce.6.cloned.1.call-done = f32[512,1024]{1,0:T(8,128)} async-done(((f32[512,1024]{1,0:T(8,128)}), f32[512,1024]{1,0:T(8,128)}) %all-reduce.6.cloned.1.call-update) | async-done | bytes 2097168 | tf_op jit(solution)/shard_map/psum | solution.py:52
  510.8 0.0 copy-start
  510.8 2.0 multiply_reduce_fusion
  512.8 11.7 %psum.23 = f32[512]{0:T(512)S(1)} all-reduce(f32[512]{0:T(512)S(1)} %multiply_reduce_fusion), channel_id=1, replica_groups=mesh['ra'=4,'cb'=4,'dp'=2] {'ra'}, use_global_device_ids=true, to_apply=%region_4.0 | all-reduce | flops 512 | bytes 4096 | tf_op jit(solution)/shard_map/psum | solution.py:53
  524.5 0.0 copy-done.4
  524.5 0.0 copy-done
  524.5 1.4 fusion.15
  (2 shorter events, 0.0 us)
Async XLA Ops:
  14.8 133.8 %all-to-all-start.1 = ((bf16[1024,4,704]{0,2,1:T(8,128)(2,1)}), bf16[1024,4,704]{0,2,1:T(8,128)(2,1)}, u32[]{:S(2)}, u32[]{:S(2)}) async-start(bf16[1024,4,704]{0,2,1:T(8,128)(2,1)} %bitcast.26), calls=%async_computation.1 | async-start | bytes 11534336 | tf_op jit(solution)/shard_map/all_to_all | solution.py:31
  148.6 5.3 %copy-start.2 = (bf16[1,512,1024]{2,1,0:T(8,128)(2,1)S(1)}, bf16[1,512,1024]{2,1,0:T(8,128)(2,1)}, u32[]{:S(2)}) copy-start(bf16[1,512,1024]{2,1,0:T(8,128)(2,1)} %param.8) | copy-start | bytes 3145732
  148.6 5.4 %copy-start.3 = (f32[1024]{0:T(1024)S(1)}, f32[1024]{0:T(1024)}, u32[]{:S(2)}) copy-start(f32[1024]{0:T(1024)} %param.9) | copy-start | bytes 12292
  148.6 199.5 %all-to-all-start = ((bf16[1024,4,704]{0,2,1:T(8,128)(2,1)}), bf16[1024,4,704]{0,2,1:T(8,128)(2,1)}, u32[]{:S(2)}, u32[]{:S(2)}) async-start(bf16[1024,4,704]{0,2,1:T(8,128)(2,1)} %bitcast.25), calls=%async_computation | async-start | bytes 11534336 | tf_op jit(solution)/shard_map/all_to_all | solution.py:30
  153.9 200.4 %all-gather.3.cloned.1.call-start = ((), (), s32[]{:S(2)}) async-start(), calls=%async_computation.2 | async-start | bytes 5242880 | tf_op jit(solution)/shard_map/all_gather | solution.py:34
  155.3 279.2 %all-gather.5.cloned.1.call-start = ((), (), s32[]{:S(2)}) async-start(), calls=%async_computation.3 | async-start | bytes 3604480 | tf_op jit(solution)/shard_map/all_gather | solution.py:47
  354.3 6.6 %copy-start.1 = (bf16[4,88,8,1024]{3,2,0,1:T(8,128)(2,1)S(1)}, bf16[4,88,8,1024]{3,2,0,1:T(8,128)(2,1)}, u32[]{:S(2)}) copy-start(bf16[4,88,8,1024]{3,2,0,1:T(8,128)(2,1)} %copy.13) | copy-start | bytes 17301508
  354.3 6.8 %copy-start.5 = (bf16[512,4096]{1,0:T(8,128)(2,1)S(1)}, bf16[512,4096]{1,0:T(8,128)(2,1)}, u32[]{:S(2)}) copy-start(bf16[512,4096]{1,0:T(8,128)(2,1)} %all-gather.3.cloned.1.call-done) | copy-start | bytes 12582916
  368.0 142.8 %all-reduce.6.cloned.1.call-start = ((), (), s32[]{:S(2)}) async-start(), calls=%async_computation.4 | async-start | bytes 4194304 | tf_op jit(solution)/shard_map/psum | solution.py:52
  442.5 82.0 %copy-start.4 = (f32[1024]{0:T(1024)S(1)}, f32[1024]{0:T(1024)}, u32[]{:S(2)}) copy-start(f32[1024]{0:T(1024)} %param.15) | copy-start | bytes 12292
  510.8 13.7 %copy-start = (f32[512,1024]{1,0:T(8,128)S(1)}, f32[512,1024]{1,0:T(8,128)}, u32[]{:S(2)}) copy-start(f32[512,1024]{1,0:T(8,128)} %all-reduce.6.cloned.1.call-done) | copy-start | bytes 6291460
Sparse Core Ops, SparseCore 0:
  156.3 164.8 all-gather.2
  368.2 66.2 all-gather.4
  442.6 68.1 all-reduce.5
where the time goes:
time: 533 us; the launch traced here: 532 us
  waiting for transfers between devices  276 us (52%)
  blocking collectives  175 us (33%)
  local copies, waits for them, and re-layouts  31 us (6%)
  matrix products  17.8 us (3%)
  between operations  13.2 us (2%)
  starting transfers between devices  11.8 us (2%)
  other arithmetic  7.39 us (1%)
    psum x1, blocking collectives, local(): total_sq = lax.psum(local_sq, 'ra')  164 us
    all_to_all x1, waiting for transfers between devices, local(): lax.all_to_all(w_up, 'ra', split_axis=1, concat_axis=0, tiled=True)  119 us
    psum x1, waiting for transfers between devices, local(): branch = lax.psum(partial_value, 'cb')  68.3 us
    all_gather x1, waiting for transfers between devices, local(): lax.all_gather(hidden, 'ra', axis=0, tiled=True)  66.4 us
    all_to_all x1, waiting for transfers between devices, local(): lax.all_to_all(w_gate, 'ra', split_axis=1, concat_axis=0, tiled=True)  22 us
    unnamed x14, local copies, waits for them, and re-layouts  16.7 us
    psum x1, blocking collectives, local(): post_sq = lax.psum(jnp.sum(branch * branch, axis=1), 'ra')  11.7 us
  transfers between devices with their start and end apart: 5, of which 4 were waited for; matrix products, arithmetic and copies ran while one was open for 4% of the time, Pallas kernels for 0%

commit v1 on v0

--- a/solution.py
+++ b/solution.py
@@ -26,15 +26,17 @@
     total_sq = lax.psum(local_sq, "ra")
     in_scale = lax.rsqrt(total_sq / dim_full + epsilon)
     weighted = (values * pre_gain).astype(jnp.bfloat16)
-    gate_cols, up_cols = (
-        lax.all_to_all(w_gate, "ra", split_axis=1, concat_axis=0, tiled=True),
-        lax.all_to_all(w_up, "ra", split_axis=1, concat_axis=0, tiled=True),
-    )
-    own_units = gate_cols.shape[1]
-    piece = lax.all_gather(weighted, "ra", axis=1, tiled=True)
+    wire = jnp.bfloat16 if ra_count <= 4 else jnp.float32
     dims = (((0,), (1,)), ((), ()))
-    gate_sum = lax.dot_general(gate_cols, piece, dims, preferred_element_type=jnp.float32)
-    up_sum = lax.dot_general(up_cols, piece, dims, preferred_element_type=jnp.float32)
+
+    def summed(weights):
+        part = lax.dot_general(weights, weighted, dims, preferred_element_type=jnp.float32)
+        full = lax.psum_scatter(part.astype(wire), "ra", scatter_dimension=0, tiled=True)
+        return full.astype(jnp.float32)
+
+    gate_sum = summed(w_gate)
+    up_sum = summed(w_up)
+    own_units = gate_sum.shape[0]
     offset_units = lax.axis_index("ra") * own_units
     taps_gate = lax.dynamic_slice_in_dim(conv_gate, offset_units, own_units, 1)
     taps_up = lax.dynamic_slice_in_dim(conv_up, offset_units, own_units, 1)
@@ -49,11 +51,13 @@
         (((0,), (0,)), ((), ())),
         preferred_element_type=jnp.float32,
     )
-    branch = lax.psum(partial_value, "cb")
+    branch = lax.psum_scatter(partial_value, "cb", scatter_dimension=0, tiled=True)
+    rows = branch.shape[0]
+    own = lax.dynamic_slice_in_dim(values, lax.axis_index("cb") * rows, rows, 0)
     post_sq = lax.psum(jnp.sum(branch * branch, axis=1), "ra")
     post_scale = lax.rsqrt(post_sq / dim_full + epsilon)
-    mixed = residual_scale * values + branch * post_scale[:, None] * post_gain
-    return mixed.astype(jnp.bfloat16)[None]
+    mixed = residual_scale * own + branch * post_scale[:, None] * post_gain
+    return lax.all_gather(mixed.astype(jnp.bfloat16), "cb", axis=0, tiled=True)[None]
 
 
 def solution(mesh):

time: 533 us -> 287 us (0.54)
  blocking collectives: 175 us -> 25.5 us
  waiting for transfers between devices: 276 us -> 205 us
  local copies, waits for them, and re-layouts: 31 us -> 16.4 us
  starting transfers between devices: 11.8 us -> 0.17 us
    psum x1, blocking collectives: 164 us -> 13.8 us  [local(): total_sq = lax.psum(local_sq, 'ra')]
    all_to_all x2 -> x0, waiting for transfers between devices: 141 us -> none  [the longest x1 119 us: local(): lax.all_to_all(w_up, 'ra', split_axis=1, concat_axis=0, tiled=True)]
    unnamed x3 -> x7, waiting for transfers between devices: 0.05 us -> 88.3 us
    psum x1 -> x0, waiting for transfers between devices: 68.3 us -> none  [local(): branch = lax.psum(partial_value, 'cb')]
    reduce_scatter x0 -> x1, waiting for transfers between devices: none -> 33.7 us  [local(): lax.psum_scatter(partial_value, 'cb', scatter_dimension=0, tiled=True)]
    all_gather x1, waiting for transfers between devices: 0.01 us -> 23.9 us  [local(): lax.all_gather(mixed.astype(jnp.bfloat16), 'cb', axis=0, tiled=True)[None]]
    all_to_all x2 -> x0, local copies, waits for them, and re-layouts: 12.2 us -> none  [the longest x1 6.14 us: local(): lax.all_to_all(w_gate, 'ra', split_axis=1, concat_axis=0, tiled=True)]
    all_to_all x2 -> x0, starting transfers between devices: 11.6 us -> none  [the longest x1 6.35 us: local(): lax.all_to_all(w_up, 'ra', split_axis=1, concat_axis=0, tiled=True)]
  transfers between devices with their start and end apart: 5 -> 5, of which waited for: 4 -> 5; matrix products, arithmetic and copies ran while one was open for 4% -> 5% of each run, Pallas kernels for 0% -> 0%
where the time goes in v1:
time: 287 us
  waiting for transfers between devices  205 us (71%)
  blocking collectives  25.5 us (9%)
  matrix products  21.3 us (7%)
  local copies, waits for them, and re-layouts  16.4 us (6%)
  between operations  13.2 us (5%)
  other arithmetic  5.51 us (2%)
    unnamed x7, waiting for transfers between devices  88.3 us
    all_gather x1, waiting for transfers between devices, local(): lax.all_gather(hidden, 'ra', axis=0, tiled=True)  59 us
    reduce_scatter x1, waiting for transfers between devices, local(): lax.psum_scatter(partial_value, 'cb', scatter_dimension=0, tiled=True)  33.7 us
    all_gather x1, waiting for transfers between devices, local(): lax.all_gather(mixed.astype(jnp.bfloat16), 'cb', axis=0, tiled=True)[None]  23.9 us
    unnamed x11, local copies, waits for them, and re-layouts  13.8 us
    psum x1, blocking collectives, local(): total_sq = lax.psum(local_sq, 'ra')  13.8 us
    dot_general x2, matrix products, summed(): lax.dot_general(weights, weighted, dims, preferred_element_type=jnp.float32)  13.3 us
    psum x1, blocking collectives, local(): post_sq = lax.psum(jnp.sum(branch * branch, axis=1), 'ra')  11.7 us
  transfers between devices with their start and end apart: 5, of which 5 were waited for; matrix products, arithmetic and copies ran while one was open for 5% of the time, Pallas kernels for 0%

profile of v1, /device:TPU:0, one launch (start us, length us, event | category | flops | bytes accessed | tf_op | source)
XLA Modules:
  0.0 286.9 jit_solution(4941577998384386182)
XLA Ops:
  6.5 0.0 reduce-scatter.10.cloned.1.call-start
  6.5 6.1 %fusion = bf16[2816,512]{0,1:T(8,128)(2,1)S(1)} fusion(bf16[1024,2816]{1,0:T(8,128)(2,1)} %param.10, f32[1024]{0:T(1024)} %param.9, bf16[1,512,1024]{2,1,0:T(8,128)(2,1)} %param.8), kind=kOutput, calls=%fused_computation.2 | convolution fusion | flops 2955804672 | bytes 9703424 | tf_op jit(solution)/shard_map/dot_general | solution.py:33
  12.7 2.8 copy.10
  15.5 0.0 copy-start
  15.5 0.0 copy-start.2
  15.5 0.0 reduce-scatter.10.cloned.1.call-update
  15.6 0.0 reduce-scatter.12.cloned.1.call-start
  15.6 1.1 copy-done
  16.8 0.0 copy-done.2
  16.8 7.1 %fusion.1 = bf16[2816,512]{0,1:T(8,128)(2,1)} fusion(bf16[1024,2816]{1,0:T(8,128)(2,1)} %param.11, f32[1024]{0:T(1024)S(1)} %copy-done.2, bf16[1,512,1024]{2,1,0:T(8,128)(2,1)S(1)} %copy-done), kind=kOutput, calls=%fused_computation.3 | convolution fusion | flops 2955804672 | bytes 9703424 | tf_op jit(solution)/shard_map/dot_general | solution.py:33
  23.9 4.8 %copy.12 = bf16[2816,512]{1,0:T(8,128)(2,1)} copy(bf16[2816,512]{0,1:T(8,128)(2,1)} %fusion.1) | data formatting | bytes 5767168
  28.7 0.0 reduce-scatter.12.cloned.1.call-update
  28.7 0.0 all-gather.3.cloned.1.call-start
  28.8 1.0 dynamic-slice_reduce_fusion.2
  29.7 0.3 fusion.3
  30.0 13.8 %psum.14 = f32[512]{0:T(512)S(1)} all-reduce(f32[512]{0:T(512)S(1)} %fusion.3), channel_id=1, replica_groups=mesh['ra'=4,'cb'=4,'dp'=2] {'ra'}, use_global_device_ids=true, to_apply=%region_2.0 | all-reduce | flops 512 | bytes 4096 | tf_op jit(solution)/shard_map/psum | solution.py:26
  43.8 31.2 %reduce-scatter.10.cloned.1.call-done = bf16[704,512]{1,0:T(8,128)(2,1)} async-done(((bf16[2816,512]{1,0:T(8,128)(2,1)}), bf16[704,512]{1,0:T(8,128)(2,1)}) %reduce-scatter.10.cloned.1.call-update) | async-done | bytes 720912
  75.0 1.4 copy.11
  76.4 57.0 %reduce-scatter.12.cloned.1.call-done = bf16[704,512]{1,0:T(8,128)(2,1)} async-done(((bf16[2816,512]{1,0:T(8,128)(2,1)}), bf16[704,512]{1,0:T(8,128)(2,1)}) %reduce-scatter.12.cloned.1.call-update) | async-done | bytes 720912
  133.4 1.4 copy.13
  134.8 0.3 convert_multiply_fusion.1
  135.1 0.5 fusion.16
  135.5 1.7 fusion.12
  137.2 1.1 copy.9
  138.3 0.0 all-gather.3.cloned.1.call-update
  138.3 0.0 reduce-scatter.8.cloned.1.call-start
  138.4 59.0 %all-gather.3.cloned.1.call-done = bf16[2816,512]{1,0:T(8,128)(2,1)} async-done(((bf16[704,512]{1,0:T(8,128)(2,1)}), bf16[2816,512]{1,0:T(8,128)(2,1)}) %all-gather.3.cloned.1.call-update) | async-done | bytes 2883600 | tf_op jit(solution)/shard_map/all_gather | solution.py:49
  197.4 8.0 %fusion.18 = f32[512,1024]{1,0:T(8,128)} fusion(bf16[2816,512]{1,0:T(8,128)(2,1)} %all-gather.3.cloned.1.call-done, bf16[2816,1024]{1,0:T(8,128)(2,1)} %param.14), kind=kOutput, calls=%fused_computation.33 | convolution fusion | flops 2952790016 | bytes 10747904 | tf_op jit(solution)/shard_map/dot_general | solution.py:48
  205.4 0.0 reduce-scatter.8.cloned.1.call-update
  205.4 0.0 copy-start.1
  205.4 0.0 all-gather.5.cloned.1.call-start
  205.5 0.2 convert_element_type.33
  205.7 33.7 %reduce-scatter.8.cloned.1.call-done = f32[128,1024]{1,0:T(8,128)} async-done(((f32[512,1024]{1,0:T(8,128)}), f32[128,1024]{1,0:T(8,128)}) %reduce-scatter.8.cloned.1.call-update) | async-done | bytes 524304 | tf_op jit(solution)/shard_map/reduce_scatter | solution.py:54
  239.4 1.2 multiply_reduce_fusion
  240.6 11.7 %psum.15 = f32[128]{0:T(128)S(1)} all-reduce(f32[128]{0:T(128)S(1)} %multiply_reduce_fusion), channel_id=1, replica_groups=mesh['ra'=4,'cb'=4,'dp'=2] {'ra'}, use_global_device_ids=true, to_apply=%region_6.0 | all-reduce | flops 128 | bytes 1024 | tf_op jit(solution)/shard_map/psum | solution.py:57
  252.3 0.0 copy-done.1
  252.3 1.9 fusion.15
  254.2 0.0 all-gather.5.cloned.1.call-update
  254.2 23.9 %all-gather.5.cloned.1.call-done = bf16[512,1024]{1,0:T(8,128)(2,1)} async-done(((bf16[128,1024]{1,0:T(8,128)(2,1)}), bf16[512,1024]{1,0:T(8,128)(2,1)}) %all-gather.5.cloned.1.call-update) | async-done | bytes 1048592 | tf_op jit(solution)/shard_map/all_gather | solution.py:60
  278.1 2.3 copy.15
  (2 shorter events, 0.0 us)
Async XLA Ops:
  6.5 68.5 %reduce-scatter.10.cloned.1.call-start = ((), (), s32[]{:S(2)}) async-start(), calls=%async_computation.6 | async-start | bytes 3604480
  15.5 1.2 copy-start
  15.5 1.2 copy-start.2
  15.6 117.8 %reduce-scatter.12.cloned.1.call-start = ((), (), s32[]{:S(2)}) async-start(), calls=%async_computation.7 | async-start | bytes 3604480
  28.7 168.7 %all-gather.3.cloned.1.call-start = ((), (), s32[]{:S(2)}) async-start(), calls=%async_computation.3 | async-start | bytes 3604480 | tf_op jit(solution)/shard_map/all_gather | solution.py:49
  138.3 101.1 %reduce-scatter.8.cloned.1.call-start = ((), (), s32[]{:S(2)}) async-start(), calls=%async_computation.4 | async-start | bytes 2621440 | tf_op jit(solution)/shard_map/reduce_scatter | solution.py:54
  205.4 46.9 %copy-start.1 = (f32[1024]{0:T(1024)S(1)}, f32[1024]{0:T(1024)}, u32[]{:S(2)}) copy-start(f32[1024]{0:T(1024)} %param.15) | copy-start | bytes 12292
  205.4 72.7 %all-gather.5.cloned.1.call-start = ((), (), s32[]{:S(2)}) async-start(), calls=%async_computation.5 | async-start | bytes 1310720 | tf_op jit(solution)/shard_map/all_gather | solution.py:60
Sparse Core Ops, SparseCore 0:
  15.7 59.2 reduce-scatter.9
  77.3 56.0 reduce-scatter.11
  138.5 58.8 all-gather.2
  205.5 33.8 reduce-scatter.7
  254.3 23.7 all-gather.4

commit v2 on v0

v2 whole, which is shorter than its diff:
```python
import functools
import jax
import jax.numpy as jnp
from jax import lax
from jax.experimental import pallas as pl
from jax.experimental.pallas import tpu as pltpu
from jax.sharding import PartitionSpec as P

epsilon = 1e-06
residual_scale = 0.125
LANES = 128
MESH = pl.DeviceIdType.MESH


def gelu(v):
    return 0.5 * v * (1.0 + jnp.tanh(0.7978845608028654 * (v + 0.044715 * v * v * v)))


def kernel(
    n, m, wire,
    tok_ref, pre_ref, wg_hbm, wu_hbm, cg_ref, cu_ref, wd_hbm, post_ref, out_ref,
    wg, wu, wd, xw, gu, rbuf, sbuf, hid, acc, sq_out, sq_in, scale, bsend, brecv, ps_out, ps_in,
    wsem, dsem, psend, precv, hsend, hrecv, sqs, sqr, bss, bsr, pss, psr, oss, osr,
):
    rows, width = tok_ref.shape
    chunks = rbuf.shape[1]
    half = chunks * LANES
    block = rows // m
    dim_full = width * n
    r = lax.axis_index("ra")
    me = lax.axis_index("cb")
    f32, bf16 = jnp.float32, jnp.bfloat16

    def units(d, c):
        return pl.ds(pl.multiple_of(d * half + c * LANES, LANES), LANES)

    def weight_copies(d, c):
        at = units(d, c)
        return (
            pltpu.make_async_copy(wg_hbm.at[:, at], wg.at[:, at], wsem.at[0, d, c]),
            pltpu.make_async_copy(wu_hbm.at[:, at], wu.at[:, at], wsem.at[1, d, c]),
        )

    first = (2 * r) // n

    def fetch(c, carry):
        for i in (0, 1):
            for copy in weight_copies((i + first) % 2, c):
                copy.start()
        return carry

    lax.fori_loop(0, chunks, fetch, 0)
    down_copy = pltpu.make_async_copy(wd_hbm, wd, dsem)
    down_copy.start()

    barrier = pltpu.get_barrier_semaphore()
    for k in range(1, n):
        pl.semaphore_signal(barrier, inc=1, device_id={"ra": (r + k) % n}, device_id_type=MESH)
    for k in range(1, m):
        pl.semaphore_signal(barrier, inc=1, device_id={"cb": (me + k) % m}, device_id_type=MESH)

    values = tok_ref[...].astype(f32)
    xw[...] = (values * pre_ref[...]).astype(bf16)
    square = values * values
    high = square.astype(bf16)
    low = (square - high.astype(f32)).astype(bf16)
    ones = jnp.ones((8, width), bf16)
    nt = (((1,), (1,)), ((), ()))
    sq_out[...] = lax.dot_general(ones, high, nt, preferred_element_type=f32) + lax.dot_general(
        ones, low, nt, preferred_element_type=f32
    )
    acc[...] = jnp.zeros_like(acc)
    pl.semaphore_wait(barrier, n - 1 + m - 1)

    def square_copy(end, k):
        return pltpu.make_async_remote_copy(
            src_ref=sq_out, dst_ref=sq_in.at[k],
            send_sem=sqs.at[end], recv_sem=sqr.at[k],
            device_id={"ra": end * (n - 1)}, device_id_type=MESH,
        )

    for end in (0, 1):
        @pl.when(r != end * (n - 1))
        def _():
            square_copy(end, r).start()

    def partial_copy(d, c):
        return pltpu.make_async_remote_copy(
            src_ref=sbuf.at[d, c], dst_ref=rbuf.at[d, c],
            send_sem=psend.at[d, c], recv_sem=precv.at[d, c],
            device_id={"ra": (r + 1 - 2 * d + n) % n}, device_id_type=MESH,
        )

    def hidden_copy(d, c):
        return pltpu.make_async_remote_copy(
            src_ref=hid.at[d, c], dst_ref=hid.at[d, c],
            send_sem=hsend.at[d, c], recv_sem=hrecv.at[d, c],
            device_id={"ra": (r - 1 + 2 * d + n) % n}, device_id_type=MESH,
        )

    def place(d):
        return r * (1 - d) + (n - 1 - r) * d

    def total_scale():
        total = sq_out[...]
        for k in range(n):
            @pl.when(r != k)
            def _():
                square_copy(0, k).wait_recv()
            total = total + jnp.where(r != k, sq_in[k], 0.0)
        inv = lax.rsqrt(total / dim_full + epsilon)
        scale[...] = jnp.concatenate([inv] * (LANES // 8), axis=0).T

    def convolve(field, taps_ref, at):
        spot = lax.broadcasted_iota(jnp.int32, field.shape, 0)
        before = jnp.where(spot == 0, 0.0, pltpu.roll(field, 1, 0))
        after = jnp.where(spot == rows - 1, 0.0, pltpu.roll(field, rows - 1, 0))
        return taps_ref[0:1, at] * before + taps_ref[1:2, at] * field + taps_ref[2:3, at] * after

    def step(s, carry):
        for i in (0, 1):
            d = (i + first) % 2
            p = place(d)
            c = s - p

            @pl.when((c >= 0) & (c < chunks))
            def _():
                at = units(d, c)
                for copy in weight_copies(d, c):
                    copy.wait()
                gu[:, :LANES] = jnp.dot(xw[...], wg[:, at], preferred_element_type=f32)
                gu[:, LANES:] = jnp.dot(xw[...], wu[:, at], preferred_element_type=f32)

                @pl.when(p == 0)
                def _():
                    sbuf[d, c] = gu[...].astype(wire)
                    partial_copy(d, c).start()

                @pl.when(p > 0)
                def _():
                    partial_copy(d, c).wait_recv()

                @pl.when((p > 0) & (p < n - 1))
                def _():
                    sbuf[d, c] = (gu[...] + rbuf[d, c].astype(f32)).astype(wire)
                    partial_copy(d, c).start()

                @pl.when(p == n - 1)
                def _():
                    @pl.when(c == 0)
                    def _():
                        total_scale()

                    by = scale[...]
                    gate_lin = (gu[:, :LANES] + rbuf[d, c, :, :LANES].astype(f32)) * by
                    up_lin = (gu[:, LANES:] + rbuf[d, c, :, LANES:].astype(f32)) * by
                    gate_conv = convolve(gate_lin, cg_ref, at)
                    up_conv = convolve(up_lin, cu_ref, at)
                    hid[d, c] = (gelu(gate_conv) * up_conv).astype(bf16)
                    hidden_copy(d, c).start()

        @pl.when(s == n - 1)
        def _():
            down_copy.wait()

        for i in (0, 1):
            d = (1 - i + first) % 2
            p = place(d)
            c = s - 2 * (n - 1) + p

            @pl.when((c >= 0) & (c < chunks))
            def _():
                @pl.when(p < n - 1)
                def _():
                    hidden_copy(d, c).wait_recv()

                @pl.when((p > 0) & (p < n - 1))
                def _():
                    hidden_copy(d, c).start()

                acc[...] += jnp.dot(hid[d, c], wd[units(d, c), :], preferred_element_type=f32)

        return carry

    lax.fori_loop(0, chunks + 2 * (n - 1), step, 0)

    bsend[...] = acc[...].astype(wire)

    def rows_of(j):
        return pl.ds(pl.multiple_of(j * block, block), block)

    def branch_copy(k):
        peer = (me + k) % m
        return pltpu.make_async_remote_copy(
            src_ref=bsend.at[rows_of(peer)], dst_ref=brecv.at[k],
            send_sem=bss.at[k], recv_sem=bsr.at[k],
            device_id={"cb": peer}, device_id_type=MESH,
        )

    for k in range(1, m):
        branch_copy(k).start()
    for k in range(1, m):
        branch_copy(k).wait_recv()
    mine = rows_of(me)
    branch = acc[mine, :]
    for k in range(1, m):
        branch = branch + brecv[k].astype(f32)
    acc[mine, :] = branch
    ps_out[...] = jnp.broadcast_to(jnp.sum(branch * branch, axis=1, keepdims=True), (block, LANES))

    def post_copy(k):
        return pltpu.make_async_remote_copy(
            src_ref=ps_out, dst_ref=ps_in.at[k],
            send_sem=pss.at[k], recv_sem=psr.at[k],
            device_id={"ra": (r + k) % n}, device_id_type=MESH,
        )

    for k in range(1, n):
        post_copy(k).start()

    for end in (0, 1):
        @pl.when(r != end * (n - 1))
        def _():
            square_copy(end, r).wait_send()


    def drain(c, carry):
        for d in (0, 1):
            p = place(d)

            @pl.when(p < n - 1)
            def _():
                partial_copy(d, c).wait_send()

            @pl.when(p > 0)
            def _():
                hidden_copy(d, c).wait_send()
        return carry

    lax.fori_loop(0, chunks, drain, 0)
    for k in range(1, m):
        branch_copy(k).wait_send()

    total = ps_out[...]
    for k in range(1, n):
        post_copy(k).wait_recv()
        total = total + ps_in[k]
    inv = lax.rsqrt(total[:, 0:1] / dim_full + epsilon)
    mixed = residual_scale * tok_ref[mine, :].astype(f32) + acc[mine, :] * inv * post_ref[...]
    out_ref[mine, :] = mixed.astype(bf16)

    def out_copy(k):
        return pltpu.make_async_remote_copy(
            src_ref=out_ref.at[mine], dst_ref=out_ref.at[mine],
            send_sem=oss.at[k], recv_sem=osr.at[k],
            device_id={"cb": (me + k) % m}, device_id_type=MESH,
        )

    for k in range(1, m):
        out_copy(k).start()
    for k in range(1, m):
        out_copy(k).wait()
    for k in range(1, n):
        post_copy(k).wait_send()


def local(n, m, tokens, pre_gain, w_gate, w_up, conv_gate, conv_up, w_down, post_gain):
    rows, width = tokens.shape[1:]
    total_units = w_gate.shape[1]
    chunks = total_units // (2 * LANES)
    block = rows // m
    wire = jnp.bfloat16 if n <= 4 else jnp.float32
    f32, bf16 = jnp.float32, jnp.bfloat16
    vmem = pl.BlockSpec(memory_space=pltpu.VMEM)
    hbm = pl.BlockSpec(memory_space=pl.ANY)
    dma = pltpu.SemaphoreType.DMA
    out = pl.pallas_call(
        functools.partial(kernel, n, m, wire),
        out_shape=jax.ShapeDtypeStruct((rows, width), bf16),
        in_specs=[vmem, vmem, hbm, hbm, vmem, vmem, hbm, vmem],
        out_specs=vmem,
        scratch_shapes=[
            pltpu.VMEM(w_gate.shape, bf16),
            pltpu.VMEM(w_up.shape, bf16),
            pltpu.VMEM(w_down.shape, bf16),
            pltpu.VMEM((rows, width), bf16),
            pltpu.VMEM((rows, 2 * LANES), f32),
            pltpu.VMEM((2, chunks, rows, 2 * LANES), wire),
            pltpu.VMEM((2, chunks, rows, 2 * LANES), wire),
            pltpu.VMEM((2, chunks, rows, LANES), bf16),
            pltpu.VMEM((rows, width), f32),
            pltpu.VMEM((8, rows), f32),
            pltpu.VMEM((n, 8, rows), f32),
            pltpu.VMEM((rows, LANES), f32),
            pltpu.VMEM((rows, width), wire),
            pltpu.VMEM((m, block, width), wire),
            pltpu.VMEM((block, LANES), f32),
            pltpu.VMEM((n, block, LANES), f32),
            dma((2, 2, chunks)), dma,
            dma((2, chunks)), dma((2, chunks)), dma((2, chunks)), dma((2, chunks)),
            dma((2,)), dma((n,)), dma((m,)), dma((m,)), dma((n,)), dma((n,)), dma((m,)), dma((m,)),
        ],
        compiler_params=pltpu.CompilerParams(
            collective_id=0, has_side_effects=True, vmem_limit_bytes=60 * 1024 * 1024
        ),
    )(tokens[0], pre_gain[None], w_gate, w_up, conv_gate, conv_up, w_down, post_gain[None])
    return out[None]


def solution(mesh):
    in_specs = (
        P("dp", None, "ra"),
        P("ra"),
        P("ra", "cb"),
        P("ra", "cb"),
        P(None, "cb"),
        P(None, "cb"),
        P("cb", "ra"),
        P("ra"),
    )
    out_specs = P("dp", None, "ra")
    return jax.shard_map(
        functools.partial(local, mesh.shape["ra"], mesh.shape["cb"]),
        mesh=mesh, in_specs=in_specs, out_specs=out_specs, check_vma=False,
    )
```

time: 533 us -> 151 us (0.28)
  waiting for transfers between devices: 276 us -> 0 us
  blocking collectives: 175 us -> 0 us
  Pallas kernels: 0 us -> 147 us
  local copies, waits for them, and re-layouts: 31 us -> 2.26 us
  matrix products: 17.8 us -> 0 us
  between operations: 13.2 us -> 0.01 us
  starting transfers between devices: 11.8 us -> 0 us
  other arithmetic: 7.39 us -> 0 us
    psum x2 -> x0, blocking collectives: 175 us -> none  [the longest x1 164 us: local(): total_sq = lax.psum(local_sq, 'ra')]
    pallas_call x0 -> x1, Pallas kernels: none -> 147 us  [local(): pl.pallas_call(functools.partial(kernel, n, m, wire), out_shape=jax.Shape...]
    all_to_all x2 -> x0, waiting for transfers between devices: 141 us -> none  [the longest x1 119 us: local(): lax.all_to_all(w_up, 'ra', split_axis=1, concat_axis=0, tiled=True)]
    psum x1 -> x0, waiting for transfers between devices: 68.3 us -> none  [local(): branch = lax.psum(partial_value, 'cb')]
    all_gather x2 -> x0, waiting for transfers between devices: 66.4 us -> none  [the longest x1 66.4 us: local(): lax.all_gather(hidden, 'ra', axis=0, tiled=True)]
    dot_general x3 -> x0, matrix products: 17.8 us -> none  [the longest x1 8.01 us: local(): lax.dot_general(lax.all_gather(hidden, 'ra', axis=0, tiled=True), w_down,...]
    unnamed x14 -> x1, local copies, waits for them, and re-layouts: 16.7 us -> 2.26 us
    all_to_all x2 -> x0, local copies, waits for them, and re-layouts: 12.2 us -> none  [the longest x1 6.14 us: local(): lax.all_to_all(w_gate, 'ra', split_axis=1, concat_axis=0, tiled=True)]
  transfers between devices with their start and end apart: 5 -> 0, of which waited for: 4 -> 0; matrix products, arithmetic and copies ran while one was open for 4% -> 0% of each run, Pallas kernels for 0% -> 0%
where the time goes in v2:
time: 151 us; the launch traced here: 149 us
  Pallas kernels  147 us (97%)
  local copies, waits for them, and re-layouts  2.26 us (1%)
    pallas_call x1, Pallas kernels, local(): pl.pallas_call(functools.partial(kernel, n, m, wire), out_shape=jax.Shape...  147 us

profile of v2, /device:TPU:0, one launch (start us, length us, event | category | flops | bytes accessed | tf_op | source)
XLA Modules:
  0.0 149.3 jit_solution(10509534202693964434)
XLA Ops:
  0.0 147.1 %shard_map.82 = bf16[512,1024]{1,0:T(8,128)(2,1)} custom-call(bf16[512,1024]{1,0:T(8,128)(2,1)} %bitcast.5, f32[1,1024]{1,0:T(1,128)} %bitcast.6, bf16[1024,2816]{1,0:T(8,128)(2,1)} %wg_hbm.1, bf16[1024,2816]{1,0:T(8,128)(2,1)} %wu_hbm.1, f32[3,2816]{1,0:T(4,128)} %cg_ref.1, f32[3,2816]{1,0:T(4,128)} %cu_ref.1, bf16[2816,1024]{1,0:T(8,128)(2,1)} %wd_hbm.1, ...), custom_call_target="tpu_custom_call" | custom-call | tf_op jit(solution)/shard_map/pallas_call | solution.py:277
  147.1 2.3 %copy.10 = bf16[1,512,1024]{2,1,0:T(8,128)(2,1)} copy(bf16[1,512,1024]{2,1,0:T(8,128)(2,1)} %bitcast.4) | data formatting | bytes 2097152

commit v3 on v2

--- a/solution.py
+++ b/solution.py
@@ -9,6 +9,7 @@
 epsilon = 1e-06
 residual_scale = 0.125
 LANES = 128
+HALO = 16
 MESH = pl.DeviceIdType.MESH
 
 
@@ -23,9 +24,11 @@
     wsem, dsem, psend, precv, hsend, hrecv, sqs, sqr, bss, bsr, pss, psr, oss, osr,
 ):
     rows, width = tok_ref.shape
-    chunks = rbuf.shape[1]
+    chunks = rbuf.shape[1] // 2
+    part = rows // 2
+    span = part + HALO
     half = chunks * LANES
-    block = rows // m
+    block = part // m
     dim_full = width * n
     r = lax.axis_index("ra")
     me = lax.axis_index("cb")
@@ -93,7 +96,7 @@
 
     def hidden_copy(d, c):
         return pltpu.make_async_remote_copy(
-            src_ref=hid.at[d, c], dst_ref=hid.at[d, c],
+            src_ref=hid.at[d, c, kept(c // chunks)], dst_ref=hid.at[d, c, kept(c // chunks)],
             send_sem=hsend.at[d, c], recv_sem=hrecv.at[d, c],
             device_id={"ra": (r - 1 + 2 * d + n) % n}, device_id_type=MESH,
         )
@@ -111,10 +114,16 @@
         inv = lax.rsqrt(total / dim_full + epsilon)
         scale[...] = jnp.concatenate([inv] * (LANES // 8), axis=0).T
 
-    def convolve(field, taps_ref, at):
-        spot = lax.broadcasted_iota(jnp.int32, field.shape, 0)
+    def taken(q):
+        return pl.ds(pl.multiple_of(q * (part - HALO), HALO), span)
+
+    def kept(q):
+        return pl.ds(pl.multiple_of(q * HALO, HALO), part)
+
+    def convolve(field, taps_ref, at, q):
+        spot = lax.broadcasted_iota(jnp.int32, field.shape, 0) + q * (part - HALO)
         before = jnp.where(spot == 0, 0.0, pltpu.roll(field, 1, 0))
-        after = jnp.where(spot == rows - 1, 0.0, pltpu.roll(field, rows - 1, 0))
+        after = jnp.where(spot == rows - 1, 0.0, pltpu.roll(field, span - 1, 0))
         return taps_ref[0:1, at] * before + taps_ref[1:2, at] * field + taps_ref[2:3, at] * after
 
     def step(s, carry):
@@ -123,13 +132,19 @@
             p = place(d)
             c = s - p
 
-            @pl.when((c >= 0) & (c < chunks))
-            def _():
-                at = units(d, c)
-                for copy in weight_copies(d, c):
-                    copy.wait()
-                gu[:, :LANES] = jnp.dot(xw[...], wg[:, at], preferred_element_type=f32)
-                gu[:, LANES:] = jnp.dot(xw[...], wu[:, at], preferred_element_type=f32)
+            @pl.when((c >= 0) & (c < 2 * chunks))
+            def _():
+                q = c // chunks
+                u = c % chunks
+                at = units(d, u)
+
+                @pl.when(q == 0)
+                def _():
+                    for copy in weight_copies(d, u):
+                        copy.wait()
+
+                gu[:, :LANES] = jnp.dot(xw[taken(q), :], wg[:, at], preferred_element_type=f32)
+                gu[:, LANES:] = jnp.dot(xw[taken(q), :], wu[:, at], preferred_element_type=f32)
 
                 @pl.when(p == 0)
                 def _():
@@ -151,11 +166,11 @@
                     def _():
                         total_scale()
 
-                    by = scale[...]
+                    by = scale[taken(q), :]
                     gate_lin = (gu[:, :LANES] + rbuf[d, c, :, :LANES].astype(f32)) * by
                     up_lin = (gu[:, LANES:] + rbuf[d, c, :, LANES:].astype(f32)) * by
-                    gate_conv = convolve(gate_lin, cg_ref, at)
-                    up_conv = convolve(up_lin, cu_ref, at)
+                    gate_conv = convolve(gate_lin, cg_ref, at, q)
+                    up_conv = convolve(up_lin, cu_ref, at, q)
                     hid[d, c] = (gelu(gate_conv) * up_conv).astype(bf16)
                     hidden_copy(d, c).start()
 
@@ -168,8 +183,10 @@
             p = place(d)
             c = s - 2 * (n - 1) + p
 
-            @pl.when((c >= 0) & (c < chunks))
-            def _():
+            @pl.when((c >= 0) & (c < 2 * chunks))
+            def _():
+                q = c // chunks
+
                 @pl.when(p < n - 1)
                 def _():
                     hidden_copy(d, c).wait_recv()
@@ -178,51 +195,89 @@
                 def _():
                     hidden_copy(d, c).start()
 
-                acc[...] += jnp.dot(hid[d, c], wd[units(d, c), :], preferred_element_type=f32)
+                at = pl.ds(pl.multiple_of(q * part, part), part)
+                acc[at, :] += jnp.dot(
+                    hid[d, c, kept(q), :], wd[units(d, c % chunks), :], preferred_element_type=f32
+                )
+
+        @pl.when(s == first_done)
+        def _():
+            send_branch(0)
+
+        @pl.when(s == first_done + chunks // 3)
+        def _():
+            sum_branch(0)
+
+        @pl.when(s == first_done + 2 * chunks // 3)
+        def _():
+            send_mixed(0)
 
         return carry
 
-    lax.fori_loop(0, chunks + 2 * (n - 1), step, 0)
-
-    bsend[...] = acc[...].astype(wire)
-
-    def rows_of(j):
-        return pl.ds(pl.multiple_of(j * block, block), block)
-
-    def branch_copy(k):
+    first_done = chunks - 1 + 2 * (n - 1)
+
+    def rows_of(q, j):
+        return pl.ds(pl.multiple_of(q * part + j * block, block), block)
+
+    def branch_copy(q, k):
         peer = (me + k) % m
         return pltpu.make_async_remote_copy(
-            src_ref=bsend.at[rows_of(peer)], dst_ref=brecv.at[k],
-            send_sem=bss.at[k], recv_sem=bsr.at[k],
+            src_ref=bsend.at[rows_of(q, peer)], dst_ref=brecv.at[q, k],
+            send_sem=bss.at[q, k], recv_sem=bsr.at[q, k],
             device_id={"cb": peer}, device_id_type=MESH,
         )
 
-    for k in range(1, m):
-        branch_copy(k).start()
-    for k in range(1, m):
-        branch_copy(k).wait_recv()
-    mine = rows_of(me)
-    branch = acc[mine, :]
-    for k in range(1, m):
-        branch = branch + brecv[k].astype(f32)
-    acc[mine, :] = branch
-    ps_out[...] = jnp.broadcast_to(jnp.sum(branch * branch, axis=1, keepdims=True), (block, LANES))
-
-    def post_copy(k):
-        return pltpu.make_async_remote_copy(
-            src_ref=ps_out, dst_ref=ps_in.at[k],
-            send_sem=pss.at[k], recv_sem=psr.at[k],
+    def post_copy(q, k):
+        return pltpu.make_async_remote_copy(
+            src_ref=ps_out.at[q], dst_ref=ps_in.at[q, k],
+            send_sem=pss.at[q, k], recv_sem=psr.at[q, k],
             device_id={"ra": (r + k) % n}, device_id_type=MESH,
         )
 
-    for k in range(1, n):
-        post_copy(k).start()
+    def out_copy(q, k):
+        mine = rows_of(q, me)
+        return pltpu.make_async_remote_copy(
+            src_ref=out_ref.at[mine], dst_ref=out_ref.at[mine],
+            send_sem=oss.at[q, k], recv_sem=osr.at[q, k],
+            device_id={"cb": (me + k) % m}, device_id_type=MESH,
+        )
+
+    def send_branch(q):
+        at = pl.ds(q * part, part)
+        bsend[at, :] = acc[at, :].astype(wire)
+        for k in range(1, m):
+            branch_copy(q, k).start()
+
+    def sum_branch(q):
+        mine = rows_of(q, me)
+        branch = acc[mine, :]
+        for k in range(1, m):
+            branch_copy(q, k).wait_recv()
+            branch = branch + brecv[q, k].astype(f32)
+        acc[mine, :] = branch
+        ps_out[q] = jnp.broadcast_to(jnp.sum(branch * branch, axis=1, keepdims=True), (block, LANES))
+        for k in range(1, n):
+            post_copy(q, k).start()
+
+    def send_mixed(q):
+        mine = rows_of(q, me)
+        total = ps_out[q]
+        for k in range(1, n):
+            post_copy(q, k).wait_recv()
+            total = total + ps_in[q, k]
+        inv = lax.rsqrt(total[:, 0:1] / dim_full + epsilon)
+        mixed = residual_scale * tok_ref[mine, :].astype(f32) + acc[mine, :] * inv * post_ref[...]
+        out_ref[mine, :] = mixed.astype(bf16)
+        for k in range(1, m):
+            out_copy(q, k).start()
+
+    lax.fori_loop(0, 2 * chunks + 2 * (n - 1), step, 0)
+    send_branch(1)
 
     for end in (0, 1):
         @pl.when(r != end * (n - 1))
         def _():
             square_copy(end, r).wait_send()
-
 
     def drain(c, carry):
         for d in (0, 1):
@@ -237,38 +292,23 @@
                 hidden_copy(d, c).wait_send()
         return carry
 
-    lax.fori_loop(0, chunks, drain, 0)
-    for k in range(1, m):
-        branch_copy(k).wait_send()
-
-    total = ps_out[...]
-    for k in range(1, n):
-        post_copy(k).wait_recv()
-        total = total + ps_in[k]
-    inv = lax.rsqrt(total[:, 0:1] / dim_full + epsilon)
-    mixed = residual_scale * tok_ref[mine, :].astype(f32) + acc[mine, :] * inv * post_ref[...]
-    out_ref[mine, :] = mixed.astype(bf16)
-
-    def out_copy(k):
-        return pltpu.make_async_remote_copy(
-            src_ref=out_ref.at[mine], dst_ref=out_ref.at[mine],
-            send_sem=oss.at[k], recv_sem=osr.at[k],
-            device_id={"cb": (me + k) % m}, device_id_type=MESH,
-        )
-
-    for k in range(1, m):
-        out_copy(k).start()
-    for k in range(1, m):
-        out_copy(k).wait()
-    for k in range(1, n):
-        post_copy(k).wait_send()
+    lax.fori_loop(0, 2 * chunks, drain, 0)
+    sum_branch(1)
+    send_mixed(1)
+    for q in (0, 1):
+        for k in range(1, m):
+            branch_copy(q, k).wait_send()
+            out_copy(q, k).wait()
+        for k in range(1, n):
+            post_copy(q, k).wait_send()
 
 
 def local(n, m, tokens, pre_gain, w_gate, w_up, conv_gate, conv_up, w_down, post_gain):
     rows, width = tokens.shape[1:]
     total_units = w_gate.shape[1]
     chunks = total_units // (2 * LANES)
-    block = rows // m
+    block = rows // (2 * m)
+    span = rows // 2 + HALO
     wire = jnp.bfloat16 if n <= 4 else jnp.float32
     f32, bf16 = jnp.float32, jnp.bfloat16
     vmem = pl.BlockSpec(memory_space=pltpu.VMEM)
@@ -284,21 +324,21 @@
             pltpu.VMEM(w_up.shape, bf16),
             pltpu.VMEM(w_down.shape, bf16),
             pltpu.VMEM((rows, width), bf16),
-            pltpu.VMEM((rows, 2 * LANES), f32),
-            pltpu.VMEM((2, chunks, rows, 2 * LANES), wire),
-            pltpu.VMEM((2, chunks, rows, 2 * LANES), wire),
-            pltpu.VMEM((2, chunks, rows, LANES), bf16),
+            pltpu.VMEM((span, 2 * LANES), f32),
+            pltpu.VMEM((2, 2 * chunks, span, 2 * LANES), wire),
+            pltpu.VMEM((2, 2 * chunks, span, 2 * LANES), wire),
+            pltpu.VMEM((2, 2 * chunks, span, LANES), bf16),
             pltpu.VMEM((rows, width), f32),
             pltpu.VMEM((8, rows), f32),
             pltpu.VMEM((n, 8, rows), f32),
             pltpu.VMEM((rows, LANES), f32),
             pltpu.VMEM((rows, width), wire),
-            pltpu.VMEM((m, block, width), wire),
-            pltpu.VMEM((block, LANES), f32),
-            pltpu.VMEM((n, block, LANES), f32),
+            pltpu.VMEM((2, m, block, width), wire),
+            pltpu.VMEM((2, block, LANES), f32),
+            pltpu.VMEM((2, n, block, LANES), f32),
             dma((2, 2, chunks)), dma,
-            dma((2, chunks)), dma((2, chunks)), dma((2, chunks)), dma((2, chunks)),
-            dma((2,)), dma((n,)), dma((m,)), dma((m,)), dma((n,)), dma((n,)), dma((m,)), dma((m,)),
+            dma((2, 2 * chunks)), dma((2, 2 * chunks)), dma((2, 2 * chunks)), dma((2, 2 * chunks)),
+            dma((2,)), dma((n,)), dma((2, m)), dma((2, m)), dma((2, n)), dma((2, n)), dma((2, m)), dma((2, m)),
         ],
         compiler_params=pltpu.CompilerParams(
             collective_id=0, has_side_effects=True, vmem_limit_bytes=60 * 1024 * 1024

time: 151 us -> 150 us (level)
  no operation moved by 1% of the time
where the time goes in v3:
time: 150 us; the launch traced here: 149 us
  Pallas kernels  147 us (98%)
  local copies, waits for them, and re-layouts  2.26 us (2%)
    pallas_call x1, Pallas kernels, local(): pl.pallas_call(functools.partial(kernel, n, m, wire), out_shape=jax.Shape...  147 us

profile of v3, /device:TPU:0, one launch (start us, length us, event | category | flops | bytes accessed | tf_op | source)
XLA Modules:
  0.0 149.5 jit_solution(17569617026973839269)
XLA Ops:
  0.0 147.2 %shard_map.82 = bf16[512,1024]{1,0:T(8,128)(2,1)} custom-call(bf16[512,1024]{1,0:T(8,128)(2,1)} %bitcast.5, f32[1,1024]{1,0:T(1,128)} %bitcast.6, bf16[1024,2816]{1,0:T(8,128)(2,1)} %wg_hbm.1, bf16[1024,2816]{1,0:T(8,128)(2,1)} %wu_hbm.1, f32[3,2816]{1,0:T(4,128)} %cg_ref.1, f32[3,2816]{1,0:T(4,128)} %cu_ref.1, bf16[2816,1024]{1,0:T(8,128)(2,1)} %wd_hbm.1, ...), custom_call_target="tpu_custom_call" | custom-call | tf_op jit(solution)/shard_map/pallas_call | solution.py:317
  147.2 2.3 %copy.10 = bf16[1,512,1024]{2,1,0:T(8,128)(2,1)} copy(bf16[1,512,1024]{2,1,0:T(8,128)(2,1)} %bitcast.4) | data formatting | bytes 2097152
